TPU v7x, 256 devices: a whole 4x4x8 slice. The times are simulated.
256 devices in a mesh: sp: 64 (over z, y, core), tp: 4 (over x).
Axes of the slice: x: 4, y: 4, z: 8, core: 2. Of those that a mesh axis runs over, the one named last changes fastest.
Arguments:
- residual: bfloat16 [65536, 2048], P(('sp', 'tp')), may hold values from -6 to 6
- pool_input: bfloat16 [65536, 1024], P('sp', 'tp'), may hold values from -6 to 6
- doc_ids: int32 [65536], P('sp'), may hold values from 0 to 31, never falling along the last dimension, each value on 1 to 4096 neighbouring positions
- pool_map: bfloat16 [4, 256, 256], P('tp'), may hold values from -0.375 to 0.375
- pool_scale: float32 [1024], P('tp'), may hold values from 0.1 to 1.9
- out_weight: bfloat16 [1024, 2048], replicated, may hold values from -0.1875 to 0.1875
- mix_gain: float32 [2048], replicated, may hold values from 0.1 to 1.9
- mix_shift: float32 [2048], replicated, may hold values from -1.75 to 1.75
- group_router: bfloat16 [2048, 4], replicated, may hold values from -0.125 to 0.125
- expert_router: bfloat16 [2048, 64], replicated, may hold values from -0.125 to 0.125
- expert_gate: bfloat16 [64, 2048, 512], P('sp'), may hold values from -0.375 to 0.375
- expert_up: bfloat16 [64, 2048, 512], P('sp'), may hold values from -0.375 to 0.375
- expert_down: bfloat16 [64, 512, 2048], P('sp'), may hold values from -0.75 to 0.75
- routes: int32 [65536, 2], P(('sp', 'tp')), may hold values from 0 to 63, as said below
- ffn_gain: float32 [2048], replicated, may hold values from 0.1 to 1.9
- ffn_shift: float32 [2048], replicated, may hold values from -1.75 to 1.75
Outputs:
- layer_out: bfloat16 [65536, 2048], P(('sp', 'tp'))
Inputs may be any that keep to these rules, and one draw needn't show every extreme that they name: `doc_ids`: document numbers never fall along the positions; each document has 1 to 4096 positions. `routes`: A token names 2 different experts. In each aligned block of half of one device's 256 rows, 32 experts are named exactly 8 times each and the others not at all.
All inputs are finite; a program needn't handle non-finite values.
Results may differ from a plain program's by a relative error of at most 0.0073.
Values may be sent and summed in bfloat16 or wider, within the bound.
No kernel may reach another device: no remote copies, remote signals or barrier semaphores. Data moves between devices by JAX's collectives and lax.ppermute only.
A program may use at most 128 MiB of HBM per device.

v0:
```python
import jax
import jax.numpy as jnp
from jax import lax
from jax.sharding import PartitionSpec as P

skip_scale = 2.0**0.5
epsilon = 1e-05


def from_behind(block, axis, distance):
    devices = range(lax.axis_size(axis))
    route = [(i - distance, i) for i in devices if i - distance in devices]
    return lax.ppermute(block, axis, route)


def layer_norm(values, norm_gain, norm_shift):
    center = values - jnp.mean(values, axis=-1, keepdims=True)
    spread = jnp.mean(center * center, axis=-1, keepdims=True)
    return center * lax.rsqrt(spread + epsilon) * norm_gain + norm_shift


def route_weights(normed, chosen, group_router, expert_router):
    group_logits = jnp.dot(normed, group_router, preferred_element_type=jnp.float32)
    expert_logits = jnp.dot(normed, expert_router, preferred_element_type=jnp.float32)
    group_count = group_logits.shape[1]
    expert_count = expert_logits.shape[1]
    group_exp = jnp.exp(group_logits)
    group_prob = group_exp / jnp.sum(group_exp, axis=1, keepdims=True)
    expert_ids = jnp.arange(expert_count, dtype=jnp.int32)
    picked = jnp.sum(
        jnp.where(chosen[:, :, None] == expert_ids[None, None, :], expert_logits[:, None, :], 0.0),
        axis=2,
    )
    picked_exp = jnp.exp(picked)
    pair_share = picked_exp / jnp.sum(picked_exp, axis=1, keepdims=True)
    group_of = chosen // (expert_count // group_count)
    group_ids = jnp.arange(group_count, dtype=jnp.int32)
    group_share = jnp.sum(
        jnp.where(group_of[:, :, None] == group_ids[None, None, :], group_prob[:, None, :], 0.0),
        axis=2,
    )
    return group_share * pair_share


def expert_ffn(arrived, expert_gate, expert_up, expert_down):
    sources, slot_count, width = arrived.shape
    gathered = arrived.reshape(sources * slot_count, width)
    gate_out = jnp.dot(gathered, expert_gate[0], preferred_element_type=jnp.float32)
    up_out = jnp.dot(gathered, expert_up[0], preferred_element_type=jnp.float32)
    hidden = (jax.nn.silu(gate_out) * up_out).astype(jnp.bfloat16)
    result = jnp.dot(hidden, expert_down[0], preferred_element_type=jnp.float32).astype(
        jnp.bfloat16
    )
    return result.reshape(sources, slot_count, width)


def fill_slots(normed, chosen, capacity, expert_count):
    flat_routes = chosen.reshape(-1)
    entry_count = flat_routes.shape[0]
    onehot = (flat_routes[:, None] == jnp.arange(expert_count, dtype=jnp.int32)[None, :]).astype(
        jnp.int32
    )
    slot_rank = jnp.sum((jnp.cumsum(onehot, axis=0) - onehot) * onehot, axis=1)
    slot_index = flat_routes * capacity + slot_rank
    token_ids = jnp.arange(entry_count, dtype=jnp.int32) // chosen.shape[1]
    source_row = (
        jnp.full((expert_count * capacity,), normed.shape[0], jnp.int32)
        .at[slot_index]
        .set(token_ids)
    )
    padded = jnp.concatenate([normed, jnp.zeros((1, normed.shape[1]), normed.dtype)], axis=0)
    outgoing = jnp.take(padded, source_row, axis=0).reshape(expert_count, capacity, normed.shape[1])
    return (outgoing, slot_index)


def combine_rows(returned, slot_index, weight):
    flat_out = returned.reshape(-1, returned.shape[2])
    picked = jnp.take(flat_out, slot_index, axis=0).reshape(
        weight.shape[0], weight.shape[1], flat_out.shape[1]
    )
    return jnp.sum(weight[:, :, None] * picked.astype(jnp.float32), axis=1)


def on_device(
    residual,
    pool_input,
    doc_ids,
    pool_map,
    pool_scale,
    out_weight,
    mix_gain,
    mix_shift,
    group_router,
    expert_router,
    expert_gate,
    expert_up,
    expert_down,
    routes,
    ffn_gain,
    ffn_shift,
):
    seq_rows = pool_input.shape[0]
    reach_rows = 15
    expert_count = lax.axis_size("sp")
    tp_count = lax.axis_size("tp")
    window = jnp.left_shift(jnp.int32(2), lax.axis_index("tp"))
    first_row = lax.axis_index("sp") * seq_rows
    tail_values, tail_docs = from_behind(
        (pool_input[seq_rows - reach_rows :], doc_ids[seq_rows - reach_rows :]), "sp", 1
    )
    source = jnp.concatenate([tail_values, pool_input], axis=0).astype(jnp.float32)
    all_docs = jnp.concatenate([tail_docs, doc_ids], axis=0)
    positions = first_row - reach_rows + jnp.arange(seq_rows + reach_rows, dtype=jnp.int32)
    running = jnp.zeros((seq_rows, source.shape[1]), jnp.float32)
    weight_sum = jnp.zeros((seq_rows, 1), jnp.float32)
    for offset in range(reach_rows + 1):
        begin_row = reach_rows - offset
        earlier = source[begin_row : begin_row + seq_rows]
        keep_mask = (
            (all_docs[begin_row : begin_row + seq_rows] == doc_ids)
            & (positions[begin_row : begin_row + seq_rows] >= 0)
            & (offset < window)
        )
        same_doc = keep_mask.astype(jnp.float32)[:, None]
        running = running + same_doc * earlier
        weight_sum = weight_sum + same_doc
    pooled = (running / weight_sum - source[reach_rows:]).astype(jnp.bfloat16)
    mixed = (jnp.dot(pooled, pool_map[0], preferred_element_type=jnp.float32) * pool_scale).astype(
        jnp.bfloat16
    )
    row_count = seq_rows // tp_count
    blocks = mixed.reshape(tp_count, row_count, mixed.shape[1])
    branch = jnp.einsum(
        "abc,cd->abd",
        lax.all_to_all(blocks, "tp", split_axis=0, concat_axis=2, tiled=True),
        out_weight,
        preferred_element_type=jnp.float32,
    )[0]
    normed = layer_norm(
        skip_scale * residual.astype(jnp.float32) + branch, mix_gain, mix_shift
    ).astype(jnp.bfloat16)
    weight = route_weights(normed, routes, group_router, expert_router)
    half_most = row_count * routes.shape[1] // expert_count
    half_rows = row_count // 2
    routed_parts = []
    for piece_index in range(2):
        rows_here = slice(piece_index * half_rows, (piece_index + 1) * half_rows)
        outgoing, slot_index = fill_slots(
            normed[rows_here], routes[rows_here], half_most, expert_count
        )
        returned = lax.all_to_all(
            expert_ffn(
                lax.all_to_all(outgoing, "sp", split_axis=0, concat_axis=0, tiled=True),
                expert_gate,
                expert_up,
                expert_down,
            ),
            "sp",
            split_axis=0,
            concat_axis=0,
            tiled=True,
        )
        routed_parts.append(combine_rows(returned, slot_index, weight[rows_here]))
    routed = jnp.concatenate(routed_parts, axis=0)
    return layer_norm(skip_scale * normed.astype(jnp.float32) + routed, ffn_gain, ffn_shift).astype(
        jnp.bfloat16
    )


def solution(mesh):
    in_specs = (
        P(("sp", "tp"), None),
        P("sp", "tp"),
        P("sp"),
        P("tp", None, None),
        P("tp"),
        P(),
        P(),
        P(),
        P(),
        P(),
        P("sp", None, None),
        P("sp", None, None),
        P("sp", None, None),
        P(("sp", "tp"), None),
        P(),
        P(),
    )
    out_specs = P(("sp", "tp"), None)
    return jax.shard_map(
        on_device, mesh=mesh, in_specs=in_specs, out_specs=out_specs, check_vma=False
    )
```

profile of v0, /device:TPU:8, one launch (start us, length us, event | category | flops | bytes accessed | tf_op | source)
XLA Modules:
  0.0 301.4 jit_solution(417035532456568899)
XLA Ops:
  0.0 0.9 slice.180
  0.9 1.9 collective-permute-start
  2.8 0.8 slice.182
  3.5 3.6 %collective-permute-start.1 = (s32[15]{0:T(128)S(1)}, s32[15]{0:T(128)S(1)}, u32[]{:S(2)}, u32[]{:S(2)}) collective-permute-start(s32[15]{0:T(128)S(1)} %slice.182), channel_id=1, source_target_pairs={{0,4},{4,8},{8,12},{12,16},{16,20},{20,24},{24,28},{28,32},{32,36}... | collective-permute-start | bytes 188 | tf_op jit(solution)/shard_map/ppermute | solution.py:13
  7.1 0.7 fusion.172
  8.6 0.6 reduce-window.16
  9.5 1.4 scatter_custom_fusion.1
  10.9 1.4 add_add_fusion
  12.4 1.2 maximum_convert_fusion
  13.6 4.4 %fusion.26 = bf16[1024,256]{1,0:T(8,128)(2,1)S(1)} fusion(f32[256]{0:T(256)S(1)} %copy-done.14, f32[1039,256]{1,0:T(8,128)S(1)} %maximum_convert_fusion, f32[1024]{0:T(1024)S(1)} %get-tuple-element.11, f32[1024]{0:T(1024)S(1)} %get-tuple-element.27, f32[1024]{0:T(1024)S(1)} %get-tuple-element.26, f32[1024]{0:T(1024)S(1)} %get-tuple-element.25, ...), kind=kOutput, calls=%fused_computation.37 | convolution fusion | flops 143654912 | bytes 17503232 | tf_op jit(solution)/shard_map/dot_general | solution.py:128
  18.0 1.0 copy.34
  19.0 4.3 %all-to-all-start = ((bf16[4,256,256]{1,2,0:T(8,128)(2,1)}), bf16[4,256,256]{1,2,0:T(8,128)(2,1)S(1)}, u32[]{:S(2)}, u32[]{:S(2)}) async-start(bf16[4,256,256]{1,2,0:T(8,128)(2,1)} %copy.34), calls=%async_computation | async-start | bytes 1048576 | tf_op jit(solution)/shard_map/all_to_all | solution.py:135
  23.3 9.6 %all-to-all-done = bf16[4,256,256]{1,2,0:T(8,128)(2,1)S(1)} async-done(((bf16[4,256,256]{1,2,0:T(8,128)(2,1)}), bf16[4,256,256]{1,2,0:T(8,128)(2,1)S(1)}, u32[]{:S(2)}, u32[]{:S(2)}) %all-to-all-start) | async-done | bytes 524320 | tf_op jit(solution)/shard_map/all_to_all | solution.py:135
  32.9 3.8 %fusion.173 = (f32[256]{0:T(256)S(1)}, f32[256,2048]{1,0:T(8,128)S(1)}) fusion(bf16[256,1024]{0,1:T(8,128)(2,1)S(1)} %bitcast.116, bf16[1024,2048]{1,0:T(8,128)(2,1)} %param.25, bf16[256,2048]{1,0:T(8,128)(2,1)} %param.20), kind=kOutput, calls=%fused_computation.265 | convolution fusion | flops 1075838720 | bytes 7865344 | tf_op jit(solution)/shard_map/abc,cd->abd/dot_general | solution.py:133
  36.8 0.4 multiply_reduce_fusion.3
  37.6 0.5 add_convert_fusion.1
  38.2 0.9 copy-done.3
  39.2 3.3 %gather_fusion.2 = bf16[512,2048]{1,0:T(8,128)(2,1)} fusion(bf16[129,2048]{1,0:T(8,128)(2,1)S(1)} %concatenate.18, s32[1024]{0:T(1024)S(1)} %pad_clamp_fusion.1), kind=kCustom, calls=%fused_computation.2.clone | custom fusion | bytes 4196352 | tf_op jit(solution)/shard_map/jit(_take)/gather | solution.py:72
  42.5 3.2 %select_bitcast_fusion = bf16[64,8,2048]{2,1,0:T(8,128)(2,1)} fusion(bf16[512,2048]{1,0:T(8,128)(2,1)} %gather_fusion.2, pred[512]{0:T(512)(128)(4,1)S(1)} %compare_and_fusion.1), kind=kLoop, calls=%fused_computation.26 | loop fusion | flops 1048576 | bytes 4194816 | tf_op jit(solution)/shard_map/reshape | solution.py:72
  45.6 12.1 %all-to-all-start.3 = ((bf16[64,8,2048]{2,1,0:T(8,128)(2,1)}), bf16[64,8,2048]{2,1,0:T(8,128)(2,1)}, u32[]{:S(2)}, u32[]{:S(2)}) async-start(bf16[64,8,2048]{2,1,0:T(8,128)(2,1)} %select_bitcast_fusion), calls=%async_computation.3 | async-start | bytes 4194304 | tf_op jit(solution)/shard_map/all_to_all | solution.py:153
  58.4 0.6 reduce-window.14
  59.4 1.4 scatter_custom_fusion
  60.9 1.2 slice_select_fusion
  62.0 3.3 %gather_fusion = bf16[512,2048]{1,0:T(8,128)(2,1)} fusion(bf16[129,2048]{1,0:T(8,128)(2,1)S(1)} %slice_select_fusion, s32[1024]{0:T(1024)S(1)} %pad_clamp_fusion.3), kind=kCustom, calls=%fused_computation.clone | custom fusion | bytes 4196352 | tf_op jit(solution)/shard_map/jit(_take)/gather | solution.py:72
  65.3 3.2 %select_bitcast_fusion.1 = bf16[64,8,2048]{2,1,0:T(8,128)(2,1)} fusion(bf16[512,2048]{1,0:T(8,128)(2,1)} %gather_fusion, pred[512]{0:T(512)(128)(4,1)S(1)} %compare_and_fusion.3), kind=kLoop, calls=%fused_computation.27 | loop fusion | flops 1048576 | bytes 4194816 | tf_op jit(solution)/shard_map/reshape | solution.py:72
  68.6 40.4 %all-to-all-done.3 = bf16[64,8,2048]{2,1,0:T(8,128)(2,1)} async-done(((bf16[64,8,2048]{2,1,0:T(8,128)(2,1)}), bf16[64,8,2048]{2,1,0:T(8,128)(2,1)}, u32[]{:S(2)}, u32[]{:S(2)}) %all-to-all-start.3) | async-done | bytes 2097184 | tf_op jit(solution)/shard_map/all_to_all | solution.py:153
  108.9 5.6 %all-to-all-start.1 = ((bf16[64,8,2048]{2,1,0:T(8,128)(2,1)}), bf16[64,8,2048]{2,1,0:T(8,128)(2,1)}, u32[]{:S(2)}, u32[]{:S(2)}) async-start(bf16[64,8,2048]{2,1,0:T(8,128)(2,1)} %select_bitcast_fusion.1), calls=%async_computation.1 | async-start | bytes 4194304 | tf_op jit(solution)/shard_map/all_to_all | solution.py:153
  114.6 3.5 %fusion.4 = f32[512,512]{1,0:T(8,128)S(1)} fusion(bf16[64,8,2048]{2,1,0:T(8,128)(2,1)} %all-to-all-done.3, bf16[1,2048,512]{2,1,0:T(8,128)(2,1)} %param.30), kind=kOutput, calls=%fused_computation.14 | convolution fusion | flops 1073741824 | bytes 5242880 | tf_op jit(solution)/shard_map/dot_general | solution.py:48
  118.1 6.0 %fusion.1 = bf16[64,8,2048]{2,1,0:T(8,128)(2,1)} fusion(bf16[1,512,2048]{2,1,0:T(8,128)(2,1)S(1)} %copy-done, bf16[1,2048,512]{2,1,0:T(8,128)(2,1)} %param.31, bf16[64,8,2048]{2,1,0:T(8,128)(2,1)} %all-to-all-done.3, f32[512,512]{1,0:T(8,128)S(1)} %fusion.4), kind=kOutput, calls=%fused_computation.9 | convolution fusion | flops 2150105088 | bytes 9437184 | tf_op jit(solution)/shard_map/dot_general | solution.py:51
  124.1 41.6 %all-to-all-done.1 = bf16[64,8,2048]{2,1,0:T(8,128)(2,1)} async-done(((bf16[64,8,2048]{2,1,0:T(8,128)(2,1)}), bf16[64,8,2048]{2,1,0:T(8,128)(2,1)}, u32[]{:S(2)}, u32[]{:S(2)}) %all-to-all-start.1) | async-done | bytes 2097184 | tf_op jit(solution)/shard_map/all_to_all | solution.py:153
  165.7 5.6 %all-to-all-start.4 = ((bf16[64,8,2048]{2,1,0:T(8,128)(2,1)}), bf16[64,8,2048]{2,1,0:T(8,128)(2,1)}, u32[]{:S(2)}, u32[]{:S(2)}) async-start(bf16[64,8,2048]{2,1,0:T(8,128)(2,1)} %fusion.1), calls=%async_computation.4 | async-start | bytes 4194304 | tf_op jit(solution)/shard_map/all_to_all | solution.py:151
  171.3 3.5 %fusion.12 = f32[512,512]{1,0:T(8,128)S(1)} fusion(bf16[1,2048,512]{2,1,0:T(8,128)(2,1)} %param.30, bf16[64,8,2048]{2,1,0:T(8,128)(2,1)} %all-to-all-done.1), kind=kOutput, calls=%fused_computation.22 | convolution fusion | flops 1073741824 | bytes 5242880 | tf_op jit(solution)/shard_map/dot_general | solution.py:48
  174.8 6.0 %fusion = bf16[64,8,2048]{2,1,0:T(8,128)(2,1)} fusion(bf16[1,512,2048]{2,1,0:T(8,128)(2,1)S(1)} %copy-done, bf16[1,2048,512]{2,1,0:T(8,128)(2,1)} %param.31, bf16[64,8,2048]{2,1,0:T(8,128)(2,1)} %all-to-all-done.1, f32[512,512]{1,0:T(8,128)S(1)} %fusion.12), kind=kOutput, calls=%fused_computation.8 | convolution fusion | flops 2150105088 | bytes 9437184 | tf_op jit(solution)/shard_map/dot_general | solution.py:51
  180.8 41.7 %all-to-all-done.4 = bf16[64,8,2048]{2,1,0:T(8,128)(2,1)} async-done(((bf16[64,8,2048]{2,1,0:T(8,128)(2,1)}), bf16[64,8,2048]{2,1,0:T(8,128)(2,1)}, u32[]{:S(2)}, u32[]{:S(2)}) %all-to-all-start.4) | async-done | bytes 2097184 | tf_op jit(solution)/shard_map/all_to_all | solution.py:151
  222.5 5.6 %all-to-all-start.2 = ((bf16[64,8,2048]{2,1,0:T(8,128)(2,1)}), bf16[64,8,2048]{2,1,0:T(8,128)(2,1)}, u32[]{:S(2)}, u32[]{:S(2)}) async-start(bf16[64,8,2048]{2,1,0:T(8,128)(2,1)} %fusion), calls=%async_computation.2 | async-start | bytes 4194304 | tf_op jit(solution)/shard_map/all_to_all | solution.py:151
  228.2 0.4 fusion.175
  228.8 0.4 fusion.174
  229.5 4.2 %gather_fusion.3 = bf16[256,2048]{1,0:T(8,128)(2,1)S(1)} fusion(bf16[512,2048]{1,0:T(8,128)(2,1)} %bitcast.21, s32[1024]{0:T(1024)S(1)} %pad_clamp_fusion), kind=kCustom, calls=%fused_computation.3.clone | custom fusion | bytes 2098176 | tf_op jit(solution)/shard_map/jit(_take)/gather | solution.py:78
  233.7 1.6 select_convert_fusion
  235.3 3.5 %reshape.223 = f32[128,2,2048]{2,1,0:T(2,128)} reshape(f32[256,2048]{1,0:T(8,128)} %select_convert_fusion) | data formatting | bytes 4194304 | tf_op jit(solution)/shard_map/convert_element_type | solution.py:81
  238.8 40.5 %all-to-all-done.2 = bf16[64,8,2048]{2,1,0:T(8,128)(2,1)} async-done(((bf16[64,8,2048]{2,1,0:T(8,128)(2,1)}), bf16[64,8,2048]{2,1,0:T(8,128)(2,1)}, u32[]{:S(2)}, u32[]{:S(2)}) %all-to-all-start.2) | async-done | bytes 2097184 | tf_op jit(solution)/shard_map/all_to_all | solution.py:151
  279.3 4.2 %gather_fusion.1 = bf16[256,2048]{1,0:T(8,128)(2,1)S(1)} fusion(bf16[512,2048]{1,0:T(8,128)(2,1)} %bitcast.14, s32[1024]{0:T(1024)S(1)} %pad_clamp_fusion.2), kind=kCustom, calls=%fused_computation.1.clone | custom fusion | bytes 2098176 | tf_op jit(solution)/shard_map/jit(_take)/gather | solution.py:78
  283.5 1.6 select_convert_fusion.1
  285.1 3.5 %reshape.222 = f32[128,2,2048]{2,1,0:T(2,128)} reshape(f32[256,2048]{1,0:T(8,128)} %select_convert_fusion.1) | data formatting | bytes 4194304 | tf_op jit(solution)/shard_map/convert_element_type | solution.py:81
  288.5 8.6 %multiply_reduce_fusion.1 = (f32[128,2048]{1,0:T(8,128)S(1)}, f32[128,2048]{1,0:T(8,128)S(1)}) fusion(f32[128,2,2048]{2,1,0:T(2,128)} %reshape.223, f32[128,2]{1,0:T(8,128)S(1)} %copy.40, f32[128,2,2048]{2,1,0:T(2,128)} %reshape.222, f32[128,2]{1,0:T(8,128)S(1)} %copy.35), kind=kLoop, calls=%fused_computation.30 | loop fusion | flops 1572864 | bytes 6293504 | tf_op jit(solution)/shard_map/reduce_sum | solution.py:81
  297.1 0.7 fusion.155
  297.8 0.8 multiply_reduce_fusion
  298.6 2.8 add_convert_fusion
  (80 shorter events, 3.1 us)
Async XLA Ops:
  0.0 118.0 %copy-start = (bf16[1,512,2048]{2,1,0:T(8,128)(2,1)S(1)}, bf16[1,512,2048]{2,1,0:T(8,128)(2,1)}, u32[]{:S(2)}) copy-start(bf16[1,512,2048]{2,1,0:T(8,128)(2,1)} %param.32) | copy-start | bytes 6291460
  0.0 13.5 %copy-start.14 = (f32[256]{0:T(256)S(1)}, f32[256]{0:T(256)}, u32[]{:S(2)}) copy-start(f32[256]{0:T(256)} %param.24) | copy-start | bytes 3076
  0.0 13.6 %copy-start.13 = (bf16[1,256,256]{2,1,0:T(8,128)(2,1)S(1)}, bf16[1,256,256]{2,1,0:T(8,128)(2,1)}, u32[]{:S(2)}) copy-start(bf16[1,256,256]{2,1,0:T(8,128)(2,1)} %param.23) | copy-start | bytes 393220
  0.9 11.5 %collective-permute-start = (bf16[15,256]{1,0:T(8,128)(2,1)S(1)}, bf16[15,256]{1,0:T(8,128)(2,1)S(1)}, u32[]{:S(2)}, u32[]{:S(2)}) collective-permute-start(bf16[15,256]{1,0:T(8,128)(2,1)S(1)} %slice.180), channel_id=1, source_target_pairs={{0,4},{4,8},{8,12},{12,16},{16,20},{20,24},{24,28},{28,32},{32,36}... | collective-permute-start | bytes 23048 | tf_op jit(solution)/shard_map/ppermute | solution.py:13
  3.5 7.4 %collective-permute-start.1 = (s32[15]{0:T(128)S(1)}, s32[15]{0:T(128)S(1)}, u32[]{:S(2)}, u32[]{:S(2)}) collective-permute-start(s32[15]{0:T(128)S(1)} %slice.182), channel_id=1, source_target_pairs={{0,4},{4,8},{8,12},{12,16},{16,20},{20,24},{24,28},{28,32},{32,36}... | collective-permute-start | bytes 188 | tf_op jit(solution)/shard_map/ppermute | solution.py:13
  19.0 13.9 %all-to-all-start = ((bf16[4,256,256]{1,2,0:T(8,128)(2,1)}), bf16[4,256,256]{1,2,0:T(8,128)(2,1)S(1)}, u32[]{:S(2)}, u32[]{:S(2)}) async-start(bf16[4,256,256]{1,2,0:T(8,128)(2,1)} %copy.34), calls=%async_computation | async-start | bytes 1048576 | tf_op jit(solution)/shard_map/all_to_all | solution.py:135
  36.8 1.4 copy-start.1
  36.8 0.7 copy-start.6
  36.8 0.8 copy-start.7
  38.2 1.0 copy-start.3
  45.6 15.2 %copy-start.12 = (pred[129]{0:T(512)(128)(4,1)S(1)}, pred[129]{0:T(512)(128)(4,1)}, u32[]{:S(2)}) copy-start(pred[129]{0:T(512)(128)(4,1)} %constant.119.clone.1) | copy-start | bytes 391
  45.6 63.3 %all-to-all-start.3 = ((bf16[64,8,2048]{2,1,0:T(8,128)(2,1)}), bf16[64,8,2048]{2,1,0:T(8,128)(2,1)}, u32[]{:S(2)}, u32[]{:S(2)}) async-start(bf16[64,8,2048]{2,1,0:T(8,128)(2,1)} %select_bitcast_fusion), calls=%async_computation.3 | async-start | bytes 4194304 | tf_op jit(solution)/shard_map/all_to_all | solution.py:153
  108.9 56.8 %all-to-all-start.1 = ((bf16[64,8,2048]{2,1,0:T(8,128)(2,1)}), bf16[64,8,2048]{2,1,0:T(8,128)(2,1)}, u32[]{:S(2)}, u32[]{:S(2)}) async-start(bf16[64,8,2048]{2,1,0:T(8,128)(2,1)} %select_bitcast_fusion.1), calls=%async_computation.1 | async-start | bytes 4194304 | tf_op jit(solution)/shard_map/all_to_all | solution.py:153
  165.7 56.8 %all-to-all-start.4 = ((bf16[64,8,2048]{2,1,0:T(8,128)(2,1)}), bf16[64,8,2048]{2,1,0:T(8,128)(2,1)}, u32[]{:S(2)}, u32[]{:S(2)}) async-start(bf16[64,8,2048]{2,1,0:T(8,128)(2,1)} %fusion.1), calls=%async_computation.4 | async-start | bytes 4194304 | tf_op jit(solution)/shard_map/all_to_all | solution.py:151
  180.8 47.4 %copy-start.8 = (s32[256,2]{0,1:T(2,128)S(1)}, s32[256,2]{0,1:T(2,128)}, u32[]{:S(2)}) copy-start(s32[256,2]{0,1:T(2,128)} %param.33) | copy-start | bytes 6148
  180.8 47.4 %copy-start.4 = (bf16[256,2048]{1,0:T(8,128)(2,1)S(1)}, bf16[256,2048]{1,0:T(8,128)(2,1)}, u32[]{:S(2)}) copy-start(bf16[256,2048]{1,0:T(8,128)(2,1)} %copy-done.3) | copy-start | bytes 3145732
  180.8 47.4 %copy-start.5 = (bf16[2048,64]{0,1:T(8,128)(2,1)S(1)}, bf16[2048,64]{0,1:T(8,128)(2,1)}, u32[]{:S(2)}) copy-start(bf16[2048,64]{0,1:T(8,128)(2,1)} %param.29) | copy-start | bytes 786436
  180.8 48.0 %copy-start.9 = (bf16[2048,4]{0,1:T(4,128)(2,1)S(1)}, bf16[2048,4]{0,1:T(4,128)(2,1)}, u32[]{:S(2)}) copy-start(bf16[2048,4]{0,1:T(4,128)(2,1)} %param.28) | copy-start | bytes 49156
  222.5 56.8 %all-to-all-start.2 = ((bf16[64,8,2048]{2,1,0:T(8,128)(2,1)}), bf16[64,8,2048]{2,1,0:T(8,128)(2,1)}, u32[]{:S(2)}, u32[]{:S(2)}) async-start(bf16[64,8,2048]{2,1,0:T(8,128)(2,1)} %fusion), calls=%async_computation.2 | async-start | bytes 4194304 | tf_op jit(solution)/shard_map/all_to_all | solution.py:151
  288.5 8.6 %copy-start.2 = (f32[256,2048]{1,0:T(8,128)S(1)}, f32[256,2048]{1,0:T(8,128)}, u32[]{:S(2)}) copy-start(f32[256,2048]{1,0:T(8,128)} %copy-done.1) | copy-start | bytes 6291460
  297.8 0.8 copy-start.10
  297.8 0.8 copy-start.11
where the time goes:
time: 302 us; the launch traced here: 301 us
  waiting for transfers between devices  174 us (58%)
  starting transfers between devices  38.8 us (13%)
  local copies, waits for them, and re-layouts  30.8 us (10%)
  other arithmetic  29.4 us (10%)
  matrix products  28 us (9%)
    all_to_all x2, waiting for transfers between devices, on_device(): lax.all_to_all(expert_ffn(lax.all_to_all(outgoing, 'sp', split_axis=0, co...  82.2 us
    all_to_all x2, waiting for transfers between devices, on_device(): lax.all_to_all(outgoing, 'sp', split_axis=0, concat_axis=0, tiled=True)  82 us
    all_to_all x2, starting transfers between devices, on_device(): lax.all_to_all(outgoing, 'sp', split_axis=0, concat_axis=0, tiled=True)  17.8 us
    dot_general x2, matrix products, expert_ffn(): jnp.dot(hidden, expert_down[0], preferred_element_type=jnp.float32)  12 us
    all_to_all x2, starting transfers between devices, on_device(): lax.all_to_all(expert_ffn(lax.all_to_all(outgoing, 'sp', split_axis=0, co...  11.3 us
    all_to_all x1, waiting for transfers between devices, on_device(): lax.all_to_all(blocks, 'tp', split_axis=0, concat_axis=2, tiled=True)  9.63 us
    reduce_sum x1, other arithmetic, combine_rows(): return jnp.sum(weight[:, :, None] * picked.astype(jnp.float32), axis=1)  8.57 us
    gather x2, local copies, waits for them, and re-layouts, combine_rows(): jnp.take(flat_out, slot_index, axis=0)  8.45 us
  transfers between devices with their start and end apart: 7, of which 5 were waited for; matrix products, arithmetic and copies ran while one was open for 15% of the time, Pallas kernels for 0%

commit v1 on v0

--- a/solution.py
+++ b/solution.py
@@ -132,7 +132,10 @@
     blocks = mixed.reshape(tp_count, row_count, mixed.shape[1])
     branch = jnp.einsum(
         "abc,cd->abd",
-        lax.all_to_all(blocks, "tp", split_axis=0, concat_axis=2, tiled=True),
+        jnp.concatenate(
+            lax.all_to_all(jnp.stack(jnp.split(blocks, lax.axis_size("tp"), axis=0)), "tp", 0, 0),
+            axis=2,
+        ),
         out_weight,
         preferred_element_type=jnp.float32,
     )[0]

time: 302 us -> 303 us (level)
  no operation moved by 1% of the time
where the time goes in v1:
time: 303 us; the launch traced here: 302 us
  waiting for transfers between devices  174 us (57%)
  starting transfers between devices  38.8 us (13%)
  other arithmetic  30.3 us (10%)
  local copies, waits for them, and re-layouts  30.1 us (10%)
  matrix products  28 us (9%)
    all_to_all x2, waiting for transfers between devices, on_device(): lax.all_to_all(expert_ffn(lax.all_to_all(outgoing, 'sp', split_axis=0, co...  82.2 us
    all_to_all x2, waiting for transfers between devices, on_device(): lax.all_to_all(outgoing, 'sp', split_axis=0, concat_axis=0, tiled=True)  82 us
    all_to_all x2, starting transfers between devices, on_device(): lax.all_to_all(outgoing, 'sp', split_axis=0, concat_axis=0, tiled=True)  17.8 us
    dot_general x2, matrix products, expert_ffn(): jnp.dot(hidden, expert_down[0], preferred_element_type=jnp.float32)  12 us
    all_to_all x2, starting transfers between devices, on_device(): lax.all_to_all(expert_ffn(lax.all_to_all(outgoing, 'sp', split_axis=0, co...  11.3 us
    all_to_all x1, waiting for transfers between devices, on_device(): lax.all_to_all(jnp.stack(jnp.split(blocks, lax.axis_size('tp'), axis=0)),...  9.63 us
    reduce_sum x1, other arithmetic, combine_rows(): return jnp.sum(weight[:, :, None] * picked.astype(jnp.float32), axis=1)  8.57 us
    gather x2, local copies, waits for them, and re-layouts, combine_rows(): jnp.take(flat_out, slot_index, axis=0)  8.45 us
  transfers between devices with their start and end apart: 7, of which 5 were waited for; matrix products, arithmetic and copies ran while one was open for 15% of the time, Pallas kernels for 0%

profile of v1, /device:TPU:8, one launch (start us, length us, event | category | flops | bytes accessed | tf_op | source)
XLA Modules:
  0.0 301.6 jit_solution(10519891241765402545)
XLA Ops:
  0.0 0.9 slice.184
  0.9 1.9 collective-permute-start
  2.8 0.8 slice.186
  3.5 3.6 %collective-permute-start.1 = (s32[15]{0:T(128)S(1)}, s32[15]{0:T(128)S(1)}, u32[]{:S(2)}, u32[]{:S(2)}) collective-permute-start(s32[15]{0:T(128)S(1)} %slice.186), channel_id=1, source_target_pairs={{0,4},{4,8},{8,12},{12,16},{16,20},{20,24},{24,28},{28,32},{32,36}... | collective-permute-start | bytes 188 | tf_op jit(solution)/shard_map/ppermute | solution.py:13
  7.1 0.7 fusion.172
  8.6 0.6 reduce-window.16
  9.5 1.4 scatter_custom_fusion.1
  10.9 1.4 add_add_fusion
  12.4 1.2 maximum_convert_fusion
  13.6 4.4 %fusion.26 = bf16[1024,256]{1,0:T(8,128)(2,1)S(1)} fusion(f32[256]{0:T(256)S(1)} %copy-done.14, f32[1039,256]{1,0:T(8,128)S(1)} %maximum_convert_fusion, f32[1024]{0:T(1024)S(1)} %get-tuple-element.11, f32[1024]{0:T(1024)S(1)} %get-tuple-element.27, f32[1024]{0:T(1024)S(1)} %get-tuple-element.26, f32[1024]{0:T(1024)S(1)} %get-tuple-element.25, ...), kind=kOutput, calls=%fused_computation.37 | convolution fusion | flops 143654912 | bytes 17503232 | tf_op jit(solution)/shard_map/dot_general | solution.py:128
  18.1 0.9 pad_maximum_fusion
  18.9 4.3 %all-to-all-start = ((bf16[4,1,256,256]{3,2,1,0:T(8,128)(2,1)}), bf16[4,1,256,256]{3,2,1,0:T(8,128)(2,1)S(1)}, u32[]{:S(2)}, u32[]{:S(2)}) async-start(bf16[4,1,256,256]{3,2,1,0:T(8,128)(2,1)} %pad_maximum_fusion), calls=%async_computation | async-start | bytes 1048576 | tf_op jit(solution)/shard_map/all_to_all | solution.py:136
  23.2 9.6 %all-to-all-done = bf16[4,1,256,256]{3,2,1,0:T(8,128)(2,1)S(1)} async-done(((bf16[4,1,256,256]{3,2,1,0:T(8,128)(2,1)}), bf16[4,1,256,256]{3,2,1,0:T(8,128)(2,1)S(1)}, u32[]{:S(2)}, u32[]{:S(2)}) %all-to-all-start) | async-done | bytes 524320 | tf_op jit(solution)/shard_map/all_to_all | solution.py:136
  33.1 3.8 %fusion.173 = (f32[256]{0:T(256)S(1)}, f32[256,2048]{1,0:T(8,128)S(1)}) fusion(bf16[256,1024]{0,1:T(8,128)(2,1)S(1)} %bitcast.120, bf16[1024,2048]{1,0:T(8,128)(2,1)} %param.25, bf16[256,2048]{1,0:T(8,128)(2,1)} %param.20), kind=kOutput, calls=%fused_computation.270 | convolution fusion | flops 1075838720 | bytes 7865344 | tf_op jit(solution)/shard_map/abc,cd->abd/dot_general | solution.py:133
  37.0 0.4 multiply_reduce_fusion.3
  37.7 0.5 add_convert_fusion.1
  38.3 0.9 copy-done.3
  39.3 3.3 %gather_fusion.2 = bf16[512,2048]{1,0:T(8,128)(2,1)} fusion(bf16[129,2048]{1,0:T(8,128)(2,1)S(1)} %concatenate.18, s32[1024]{0:T(1024)S(1)} %pad_clamp_fusion.1), kind=kCustom, calls=%fused_computation.2.clone | custom fusion | bytes 4196352 | tf_op jit(solution)/shard_map/jit(_take)/gather | solution.py:72
  42.6 3.2 %select_bitcast_fusion = bf16[64,8,2048]{2,1,0:T(8,128)(2,1)} fusion(bf16[512,2048]{1,0:T(8,128)(2,1)} %gather_fusion.2, pred[512]{0:T(512)(128)(4,1)S(1)} %compare_and_fusion.1), kind=kLoop, calls=%fused_computation.26 | loop fusion | flops 1048576 | bytes 4194816 | tf_op jit(solution)/shard_map/reshape | solution.py:72
  45.8 12.1 %all-to-all-start.3 = ((bf16[64,8,2048]{2,1,0:T(8,128)(2,1)}), bf16[64,8,2048]{2,1,0:T(8,128)(2,1)}, u32[]{:S(2)}, u32[]{:S(2)}) async-start(bf16[64,8,2048]{2,1,0:T(8,128)(2,1)} %select_bitcast_fusion), calls=%async_computation.3 | async-start | bytes 4194304 | tf_op jit(solution)/shard_map/all_to_all | solution.py:156
  58.6 0.6 reduce-window.14
  59.5 1.4 scatter_custom_fusion
  61.0 1.2 slice_select_fusion
  62.2 3.3 %gather_fusion = bf16[512,2048]{1,0:T(8,128)(2,1)} fusion(bf16[129,2048]{1,0:T(8,128)(2,1)S(1)} %slice_select_fusion, s32[1024]{0:T(1024)S(1)} %pad_clamp_fusion.3), kind=kCustom, calls=%fused_computation.clone | custom fusion | bytes 4196352 | tf_op jit(solution)/shard_map/jit(_take)/gather | solution.py:72
  65.5 3.2 %select_bitcast_fusion.1 = bf16[64,8,2048]{2,1,0:T(8,128)(2,1)} fusion(bf16[512,2048]{1,0:T(8,128)(2,1)} %gather_fusion, pred[512]{0:T(512)(128)(4,1)S(1)} %compare_and_fusion.3), kind=kLoop, calls=%fused_computation.27 | loop fusion | flops 1048576 | bytes 4194816 | tf_op jit(solution)/shard_map/reshape | solution.py:72
  68.7 40.4 %all-to-all-done.3 = bf16[64,8,2048]{2,1,0:T(8,128)(2,1)} async-done(((bf16[64,8,2048]{2,1,0:T(8,128)(2,1)}), bf16[64,8,2048]{2,1,0:T(8,128)(2,1)}, u32[]{:S(2)}, u32[]{:S(2)}) %all-to-all-start.3) | async-done | bytes 2097184 | tf_op jit(solution)/shard_map/all_to_all | solution.py:156
  109.1 5.6 %all-to-all-start.1 = ((bf16[64,8,2048]{2,1,0:T(8,128)(2,1)}), bf16[64,8,2048]{2,1,0:T(8,128)(2,1)}, u32[]{:S(2)}, u32[]{:S(2)}) async-start(bf16[64,8,2048]{2,1,0:T(8,128)(2,1)} %select_bitcast_fusion.1), calls=%async_computation.1 | async-start | bytes 4194304 | tf_op jit(solution)/shard_map/all_to_all | solution.py:156
  114.7 3.5 %fusion.4 = f32[512,512]{1,0:T(8,128)S(1)} fusion(bf16[64,8,2048]{2,1,0:T(8,128)(2,1)} %all-to-all-done.3, bf16[1,2048,512]{2,1,0:T(8,128)(2,1)} %param.30), kind=kOutput, calls=%fused_computation.14 | convolution fusion | flops 1073741824 | bytes 5242880 | tf_op jit(solution)/shard_map/dot_general | solution.py:48
  118.2 6.0 %fusion.1 = bf16[64,8,2048]{2,1,0:T(8,128)(2,1)} fusion(bf16[1,512,2048]{2,1,0:T(8,128)(2,1)S(1)} %copy-done, bf16[1,2048,512]{2,1,0:T(8,128)(2,1)} %param.31, bf16[64,8,2048]{2,1,0:T(8,128)(2,1)} %all-to-all-done.3, f32[512,512]{1,0:T(8,128)S(1)} %fusion.4), kind=kOutput, calls=%fused_computation.9 | convolution fusion | flops 2150105088 | bytes 9437184 | tf_op jit(solution)/shard_map/dot_general | solution.py:51
  124.2 41.7 %all-to-all-done.1 = bf16[64,8,2048]{2,1,0:T(8,128)(2,1)} async-done(((bf16[64,8,2048]{2,1,0:T(8,128)(2,1)}), bf16[64,8,2048]{2,1,0:T(8,128)(2,1)}, u32[]{:S(2)}, u32[]{:S(2)}) %all-to-all-start.1) | async-done | bytes 2097184 | tf_op jit(solution)/shard_map/all_to_all | solution.py:156
  165.9 5.6 %all-to-all-start.4 = ((bf16[64,8,2048]{2,1,0:T(8,128)(2,1)}), bf16[64,8,2048]{2,1,0:T(8,128)(2,1)}, u32[]{:S(2)}, u32[]{:S(2)}) async-start(bf16[64,8,2048]{2,1,0:T(8,128)(2,1)} %fusion.1), calls=%async_computation.4 | async-start | bytes 4194304 | tf_op jit(solution)/shard_map/all_to_all | solution.py:154
  171.5 3.5 %fusion.12 = f32[512,512]{1,0:T(8,128)S(1)} fusion(bf16[1,2048,512]{2,1,0:T(8,128)(2,1)} %param.30, bf16[64,8,2048]{2,1,0:T(8,128)(2,1)} %all-to-all-done.1), kind=kOutput, calls=%fused_computation.22 | convolution fusion | flops 1073741824 | bytes 5242880 | tf_op jit(solution)/shard_map/dot_general | solution.py:48
  174.9 6.0 %fusion = bf16[64,8,2048]{2,1,0:T(8,128)(2,1)} fusion(bf16[1,512,2048]{2,1,0:T(8,128)(2,1)S(1)} %copy-done, bf16[1,2048,512]{2,1,0:T(8,128)(2,1)} %param.31, bf16[64,8,2048]{2,1,0:T(8,128)(2,1)} %all-to-all-done.1, f32[512,512]{1,0:T(8,128)S(1)} %fusion.12), kind=kOutput, calls=%fused_computation.8 | convolution fusion | flops 2150105088 | bytes 9437184 | tf_op jit(solution)/shard_map/dot_general | solution.py:51
  180.9 41.7 %all-to-all-done.4 = bf16[64,8,2048]{2,1,0:T(8,128)(2,1)} async-done(((bf16[64,8,2048]{2,1,0:T(8,128)(2,1)}), bf16[64,8,2048]{2,1,0:T(8,128)(2,1)}, u32[]{:S(2)}, u32[]{:S(2)}) %all-to-all-start.4) | async-done | bytes 2097184 | tf_op jit(solution)/shard_map/all_to_all | solution.py:154
  222.6 5.6 %all-to-all-start.2 = ((bf16[64,8,2048]{2,1,0:T(8,128)(2,1)}), bf16[64,8,2048]{2,1,0:T(8,128)(2,1)}, u32[]{:S(2)}, u32[]{:S(2)}) async-start(bf16[64,8,2048]{2,1,0:T(8,128)(2,1)} %fusion), calls=%async_computation.2 | async-start | bytes 4194304 | tf_op jit(solution)/shard_map/all_to_all | solution.py:154
  228.4 0.4 fusion.175
  228.9 0.4 fusion.174
  229.6 4.2 %gather_fusion.3 = bf16[256,2048]{1,0:T(8,128)(2,1)S(1)} fusion(bf16[512,2048]{1,0:T(8,128)(2,1)} %bitcast.23, s32[1024]{0:T(1024)S(1)} %pad_clamp_fusion), kind=kCustom, calls=%fused_computation.3.clone | custom fusion | bytes 2098176 | tf_op jit(solution)/shard_map/jit(_take)/gather | solution.py:78
  233.8 1.6 select_convert_fusion
  235.4 3.5 %reshape.233 = f32[128,2,2048]{2,1,0:T(2,128)} reshape(f32[256,2048]{1,0:T(8,128)} %select_convert_fusion) | data formatting | bytes 4194304 | tf_op jit(solution)/shard_map/convert_element_type | solution.py:81
  238.9 40.5 %all-to-all-done.2 = bf16[64,8,2048]{2,1,0:T(8,128)(2,1)} async-done(((bf16[64,8,2048]{2,1,0:T(8,128)(2,1)}), bf16[64,8,2048]{2,1,0:T(8,128)(2,1)}, u32[]{:S(2)}, u32[]{:S(2)}) %all-to-all-start.2) | async-done | bytes 2097184 | tf_op jit(solution)/shard_map/all_to_all | solution.py:154
  279.4 4.2 %gather_fusion.1 = bf16[256,2048]{1,0:T(8,128)(2,1)S(1)} fusion(bf16[512,2048]{1,0:T(8,128)(2,1)} %bitcast.16, s32[1024]{0:T(1024)S(1)} %pad_clamp_fusion.2), kind=kCustom, calls=%fused_computation.1.clone | custom fusion | bytes 2098176 | tf_op jit(solution)/shard_map/jit(_take)/gather | solution.py:78
  283.6 1.6 select_convert_fusion.1
  285.2 3.5 %reshape.232 = f32[128,2,2048]{2,1,0:T(2,128)} reshape(f32[256,2048]{1,0:T(8,128)} %select_convert_fusion.1) | data formatting | bytes 4194304 | tf_op jit(solution)/shard_map/convert_element_type | solution.py:81
  288.7 8.6 %multiply_reduce_fusion.1 = (f32[128,2048]{1,0:T(8,128)S(1)}, f32[128,2048]{1,0:T(8,128)S(1)}) fusion(f32[128,2,2048]{2,1,0:T(2,128)} %reshape.233, f32[128,2]{1,0:T(8,128)S(1)} %copy.40, f32[128,2,2048]{2,1,0:T(2,128)} %reshape.232, f32[128,2]{1,0:T(8,128)S(1)} %copy.35), kind=kLoop, calls=%fused_computation.30 | loop fusion | flops 1572864 | bytes 6293504 | tf_op jit(solution)/shard_map/reduce_sum | solution.py:81
  297.2 0.7 fusion.155
  297.9 0.8 multiply_reduce_fusion
  298.8 2.8 add_convert_fusion
  (82 shorter events, 3.3 us)
Async XLA Ops:
  0.0 118.2 %copy-start = (bf16[1,512,2048]{2,1,0:T(8,128)(2,1)S(1)}, bf16[1,512,2048]{2,1,0:T(8,128)(2,1)}, u32[]{:S(2)}) copy-start(bf16[1,512,2048]{2,1,0:T(8,128)(2,1)} %param.32) | copy-start | bytes 6291460
  0.0 13.5 %copy-start.14 = (f32[256]{0:T(256)S(1)}, f32[256]{0:T(256)}, u32[]{:S(2)}) copy-start(f32[256]{0:T(256)} %param.24) | copy-start | bytes 3076
  0.0 13.6 %copy-start.13 = (bf16[1,256,256]{2,1,0:T(8,128)(2,1)S(1)}, bf16[1,256,256]{2,1,0:T(8,128)(2,1)}, u32[]{:S(2)}) copy-start(bf16[1,256,256]{2,1,0:T(8,128)(2,1)} %param.23) | copy-start | bytes 393220
  0.9 11.5 %collective-permute-start = (bf16[15,256]{1,0:T(8,128)(2,1)S(1)}, bf16[15,256]{1,0:T(8,128)(2,1)S(1)}, u32[]{:S(2)}, u32[]{:S(2)}) collective-permute-start(bf16[15,256]{1,0:T(8,128)(2,1)S(1)} %slice.184), channel_id=1, source_target_pairs={{0,4},{4,8},{8,12},{12,16},{16,20},{20,24},{24,28},{28,32},{32,36}... | collective-permute-start | bytes 23048 | tf_op jit(solution)/shard_map/ppermute | solution.py:13
  3.5 7.4 %collective-permute-start.1 = (s32[15]{0:T(128)S(1)}, s32[15]{0:T(128)S(1)}, u32[]{:S(2)}, u32[]{:S(2)}) collective-permute-start(s32[15]{0:T(128)S(1)} %slice.186), channel_id=1, source_target_pairs={{0,4},{4,8},{8,12},{12,16},{16,20},{20,24},{24,28},{28,32},{32,36}... | collective-permute-start | bytes 188 | tf_op jit(solution)/shard_map/ppermute | solution.py:13
  18.9 13.9 %all-to-all-start = ((bf16[4,1,256,256]{3,2,1,0:T(8,128)(2,1)}), bf16[4,1,256,256]{3,2,1,0:T(8,128)(2,1)S(1)}, u32[]{:S(2)}, u32[]{:S(2)}) async-start(bf16[4,1,256,256]{3,2,1,0:T(8,128)(2,1)} %pad_maximum_fusion), calls=%async_computation | async-start | bytes 1048576 | tf_op jit(solution)/shard_map/all_to_all | solution.py:136
  36.9 1.4 copy-start.1
  36.9 0.7 copy-start.6
  37.0 0.8 copy-start.7
  38.3 1.0 copy-start.3
  45.8 15.2 %copy-start.12 = (pred[129]{0:T(512)(128)(4,1)S(1)}, pred[129]{0:T(512)(128)(4,1)}, u32[]{:S(2)}) copy-start(pred[129]{0:T(512)(128)(4,1)} %constant.119.clone.1) | copy-start | bytes 391
  45.8 63.3 %all-to-all-start.3 = ((bf16[64,8,2048]{2,1,0:T(8,128)(2,1)}), bf16[64,8,2048]{2,1,0:T(8,128)(2,1)}, u32[]{:S(2)}, u32[]{:S(2)}) async-start(bf16[64,8,2048]{2,1,0:T(8,128)(2,1)} %select_bitcast_fusion), calls=%async_computation.3 | async-start | bytes 4194304 | tf_op jit(solution)/shard_map/all_to_all | solution.py:156
  109.1 56.8 %all-to-all-start.1 = ((bf16[64,8,2048]{2,1,0:T(8,128)(2,1)}), bf16[64,8,2048]{2,1,0:T(8,128)(2,1)}, u32[]{:S(2)}, u32[]{:S(2)}) async-start(bf16[64,8,2048]{2,1,0:T(8,128)(2,1)} %select_bitcast_fusion.1), calls=%async_computation.1 | async-start | bytes 4194304 | tf_op jit(solution)/shard_map/all_to_all | solution.py:156
  165.9 56.8 %all-to-all-start.4 = ((bf16[64,8,2048]{2,1,0:T(8,128)(2,1)}), bf16[64,8,2048]{2,1,0:T(8,128)(2,1)}, u32[]{:S(2)}, u32[]{:S(2)}) async-start(bf16[64,8,2048]{2,1,0:T(8,128)(2,1)} %fusion.1), calls=%async_computation.4 | async-start | bytes 4194304 | tf_op jit(solution)/shard_map/all_to_all | solution.py:154
  180.9 47.4 %copy-start.8 = (s32[256,2]{0,1:T(2,128)S(1)}, s32[256,2]{0,1:T(2,128)}, u32[]{:S(2)}) copy-start(s32[256,2]{0,1:T(2,128)} %param.33) | copy-start | bytes 6148
  180.9 47.4 %copy-start.4 = (bf16[256,2048]{1,0:T(8,128)(2,1)S(1)}, bf16[256,2048]{1,0:T(8,128)(2,1)}, u32[]{:S(2)}) copy-start(bf16[256,2048]{1,0:T(8,128)(2,1)} %copy-done.3) | copy-start | bytes 3145732
  180.9 47.5 %copy-start.5 = (bf16[2048,64]{0,1:T(8,128)(2,1)S(1)}, bf16[2048,64]{0,1:T(8,128)(2,1)}, u32[]{:S(2)}) copy-start(bf16[2048,64]{0,1:T(8,128)(2,1)} %param.29) | copy-start | bytes 786436
  180.9 48.0 %copy-start.9 = (bf16[2048,4]{0,1:T(4,128)(2,1)S(1)}, bf16[2048,4]{0,1:T(4,128)(2,1)}, u32[]{:S(2)}) copy-start(bf16[2048,4]{0,1:T(4,128)(2,1)} %param.28) | copy-start | bytes 49156
  222.6 56.8 %all-to-all-start.2 = ((bf16[64,8,2048]{2,1,0:T(8,128)(2,1)}), bf16[64,8,2048]{2,1,0:T(8,128)(2,1)}, u32[]{:S(2)}, u32[]{:S(2)}) async-start(bf16[64,8,2048]{2,1,0:T(8,128)(2,1)} %fusion), calls=%async_computation.2 | async-start | bytes 4194304 | tf_op jit(solution)/shard_map/all_to_all | solution.py:154
  288.7 8.6 %copy-start.2 = (f32[256,2048]{1,0:T(8,128)S(1)}, f32[256,2048]{1,0:T(8,128)}, u32[]{:S(2)}) copy-start(f32[256,2048]{1,0:T(8,128)} %copy-done.1) | copy-start | bytes 6291460
  297.9 0.8 copy-start.10
  297.9 0.8 copy-start.11
